TPU v7x, 32 devices: a whole 2x2x4 slice. The times are simulated.
32 devices in a mesh: ra: 8 (over z, y), cb: 4 (over x, core).
Axes of the slice: x: 2, y: 2, z: 4, core: 2. Of those that a mesh axis runs over, the one named last changes fastest.
Arguments:
- tokens: bfloat16 [512, 4096], P(None, 'cb'), may hold values from -400 to 400
- norm_gain: bfloat16 [4096], P('cb'), may hold values from 0.099609375 to 1.8984375
- w_gate: bfloat16 [4096, 11264], P('cb', 'ra'), may hold values from -0.09375 to 0.09375
- w_up: bfloat16 [4096, 11264], P('cb', 'ra'), may hold values from -0.09375 to 0.09375
- w_down: bfloat16 [11264, 4096], P('ra', 'cb'), may hold values from -0.0546875 to 0.0546875
- out_gain: bfloat16 [4096], P('cb'), may hold values from 0.099609375 to 1.8984375
Outputs:
- normed_out: bfloat16 [512, 4096], P('ra', 'cb')
All inputs are finite; a program needn't handle non-finite values.
Results may differ from a plain program's by a relative error of at most 0.0045.
Values sent between devices are 32-bit elements; how exact they have to be, the bound alone decides.
A program may use at most 64 MiB of HBM per device.

v0:
```python
import jax
import jax.numpy as jnp
from jax import lax
from jax.sharding import PartitionSpec as P

D = 4096


def body(tokens, norm_gain, w_gate, w_up, w_down, out_gain):
    eps = 1e-06
    xfloat = tokens.astype(jnp.float32)
    local_sq = jnp.sum(xfloat * xfloat, axis=1)
    scaled = (xfloat * norm_gain.astype(jnp.float32)).astype(jnp.bfloat16)
    gate_part = jnp.dot(scaled, w_gate, preferred_element_type=jnp.float32)
    up_part = jnp.dot(scaled, w_up, preferred_element_type=jnp.float32)
    total_sq, gate_sum, up_sum = lax.psum((local_sq, gate_part, up_part), "cb")
    inv_in = lax.rsqrt(total_sq / D + eps)[:, None]
    hidden = (jax.nn.silu(gate_sum * inv_in) * (up_sum * inv_in)).astype(jnp.bfloat16)
    partial_down = jnp.dot(hidden, w_down, preferred_element_type=jnp.float32)
    own_rows = tokens.shape[0] // lax.axis_size("ra")
    first_row = lax.axis_index("ra") * own_rows
    down = lax.psum_scatter(partial_down, "ra", scatter_dimension=0, tiled=True)
    residual = lax.dynamic_slice_in_dim(xfloat, first_row, own_rows, 0)
    mixed = 0.1 * residual + down
    out_sq = lax.psum(jnp.sum(mixed * mixed, axis=1), "cb")
    inv_out = lax.rsqrt(out_sq / D + eps)[:, None]
    return (mixed * inv_out * out_gain.astype(jnp.float32)).astype(jnp.bfloat16)


def solution(mesh):
    return jax.shard_map(
        body,
        mesh=mesh,
        in_specs=(P(None, "cb"), P("cb"), P("cb", "ra"), P("cb", "ra"), P("ra", "cb"), P("cb")),
        out_specs=P("ra", "cb"),
        check_vma=False,
    )
```

profile of v0, /device:TPU:0, one launch (start us, length us, event | category | flops | bytes accessed | tf_op | source)
XLA Modules:
  0.0 221.7 jit_solution(3549083786909565861)
XLA Ops:
  6.5 0.0 copy-start
  6.5 0.0 all-reduce.3.cloned.1.call-start
  6.5 0.8 convert_element_type.19
  7.4 1.0 copy-done
  8.4 0.0 copy-start.1
  8.4 0.0 copy-start.3
  8.4 4.7 %fusion.1 = f32[512,1408]{1,0:T(8,128)} fusion(bf16[1024,1408]{1,0:T(8,128)(2,1)S(1)} %copy-done, f32[1024]{0:T(1024)S(1)} %convert_element_type.19, bf16[512,1024]{1,0:T(8,128)(2,1)} %param.6), kind=kOutput, calls=%fused_computation.4 | convolution fusion | flops 1477967872 | bytes 6819840 | tf_op jit(solution)/shard_map/dot_general | solution.py:15
  13.1 0.0 copy-done.1
  13.1 0.0 copy-done.3
  13.1 3.5 %fusion.2 = f32[512,1408]{1,0:T(8,128)} fusion(bf16[1024,1408]{1,0:T(8,128)(2,1)S(1)} %copy-done.3, f32[1024]{0:T(1024)S(1)} %convert_element_type.19, bf16[512,1024]{1,0:T(8,128)(2,1)S(1)} %copy-done.1), kind=kOutput, calls=%fused_computation.5 | convolution fusion | flops 1477967872 | bytes 6819840 | tf_op jit(solution)/shard_map/dot_general | solution.py:14
  16.6 0.0 all-reduce.3.cloned.1.call-update
  16.6 0.0 reduce-scatter.2.cloned.1.call-start
  16.6 1.5 multiply_reduce_fusion
  18.1 8.4 %psum.29 = f32[512]{0:T(512)S(1)} all-reduce(f32[512]{0:T(512)S(1)} %multiply_reduce_fusion), channel_id=1, replica_groups=mesh['ra'=8,'cb'=4] {'cb'}, use_global_device_ids=true, to_apply=%region_2.0 | all-reduce | flops 512 | bytes 4096 | tf_op jit(solution)/shard_map/psum | solution.py:16
  26.5 104.0 %all-reduce.3.cloned.1.call-done = (f32[512,1408]{1,0:T(8,128)}, f32[512,1408]{1,0:T(8,128)}) async-done(((f32[512,1408]{1,0:T(8,128)}, f32[512,1408]{1,0:T(8,128)}), (f32[512,1408]{1,0:T(8,128)}, f32[512,1408]{1,0:T(8,128)})) %all-reduce.3.cloned.1.call-update) | async-done | bytes 5767184 | tf_op jit(solution)/shard_map/psum | solution.py:16
  130.5 6.8 %fusion = f32[512,1024]{1,0:T(8,128)} fusion(bf16[1408,1024]{1,0:T(8,128)(2,1)} %param.10, f32[512,1408]{1,0:T(8,128)} %get-tuple-element.5, f32[512,1408]{1,0:T(8,128)} %get-tuple-element.6, f32[512]{0:T(512)S(1)} %add_rsqrt_fusion), kind=kOutput, calls=%fused_computation.3 | convolution fusion | flops 1482162176 | bytes 10749952 | tf_op jit(solution)/shard_map/dot_general | solution.py:19
  137.4 0.0 copy-start.2
  137.4 0.0 reduce-scatter.2.cloned.1.call-update
  137.4 2.8 %convert_element_type.18 = f32[512,1024]{1,0:T(8,128)} convert(bf16[512,1024]{1,0:T(8,128)(2,1)} %param.6) | non-fusion elementwise | flops 524288 | bytes 3145728 | tf_op jit(solution)/shard_map/convert_element_type | solution.py:11
  140.2 0.0 copy-done.2
  140.2 66.0 %reduce-scatter.2.cloned.1.call-done = f32[64,1024]{1,0:T(8,128)} async-done(((f32[512,1024]{1,0:T(8,128)}), f32[64,1024]{1,0:T(8,128)}) %reduce-scatter.2.cloned.1.call-update) | async-done | bytes 262160 | tf_op jit(solution)/shard_map/reduce_scatter | solution.py:22
  206.2 1.2 multiply_reduce_fusion.1
  207.4 5.7 %psum.31 = f32[64]{0:T(128)S(1)} all-reduce(f32[64]{0:T(128)S(1)} %multiply_reduce_fusion.1), channel_id=1, replica_groups=mesh['ra'=8,'cb'=4] {'cb'}, use_global_device_ids=true, to_apply=%region_6.7 | all-reduce | flops 64 | bytes 512 | tf_op jit(solution)/shard_map/psum | solution.py:25
  213.0 1.8 multiply_convert_fusion.5
  (3 shorter events, 0.0 us)
Async XLA Ops:
  6.5 1.8 copy-start
  6.5 124.0 %all-reduce.3.cloned.1.call-start = ((), (), s32[]{:S(2)}) async-start(), calls=%async_computation.2 | async-start | bytes 11534336 | tf_op jit(solution)/shard_map/psum | solution.py:16
  8.4 4.7 %copy-start.1 = (bf16[512,1024]{1,0:T(8,128)(2,1)S(1)}, bf16[512,1024]{1,0:T(8,128)(2,1)}, u32[]{:S(2)}) copy-start(bf16[512,1024]{1,0:T(8,128)(2,1)} %param.6) | copy-start | bytes 3145732
  8.4 4.7 %copy-start.3 = (bf16[1024,1408]{1,0:T(8,128)(2,1)S(1)}, bf16[1024,1408]{1,0:T(8,128)(2,1)}, u32[]{:S(2)}) copy-start(bf16[1024,1408]{1,0:T(8,128)(2,1)} %param.8) | copy-start | bytes 8650756
  16.6 189.6 %reduce-scatter.2.cloned.1.call-start = ((), (), s32[]{:S(2)}) async-start(), calls=%async_computation.1 | async-start | bytes 2359296 | tf_op jit(solution)/shard_map/reduce_scatter | solution.py:22
  137.4 2.9 %copy-start.2 = (bf16[1024]{0:T(1024)(128)(2,1)S(1)}, bf16[1024]{0:T(1024)(128)(2,1)}, u32[]{:S(2)}) copy-start(bf16[1024]{0:T(1024)(128)(2,1)} %param.11) | copy-start | bytes 6148
Sparse Core Ops, SparseCore 0:
  16.7 113.7 all-reduce.2
  137.5 68.6 reduce-scatter.1
where the time goes:
time: 222 us
  waiting for transfers between devices  170 us (77%)
  matrix products  15 us (7%)
  blocking collectives  14 us (6%)
  between operations  13.4 us (6%)
  other arithmetic  8.13 us (4%)
    psum x1, waiting for transfers between devices, body(): total_sq, gate_sum, up_sum = lax.psum((local_sq, gate_part, up_part), 'cb')  104 us
    reduce_scatter x1, waiting for transfers between devices, body(): down = lax.psum_scatter(partial_down, 'ra', scatter_dimension=0, tiled=True)  66 us
    psum x1, blocking collectives, body(): total_sq, gate_sum, up_sum = lax.psum((local_sq, gate_part, up_part), 'cb')  8.37 us
    dot_general x1, matrix products, body(): partial_down = jnp.dot(hidden, w_down, preferred_element_type=jnp.float32)  6.83 us
    psum x1, blocking collectives, body(): out_sq = lax.psum(jnp.sum(mixed * mixed, axis=1), 'cb')  5.67 us
    dot_general x1, matrix products, body(): up_part = jnp.dot(scaled, w_up, preferred_element_type=jnp.float32)  4.74 us
  transfers between devices with their start and end apart: 2, of which 2 were waited for; matrix products, arithmetic and copies ran while one was open for 2% of the time, Pallas kernels for 0%

commit v1 on v0

--- a/solution.py
+++ b/solution.py
@@ -22,7 +22,7 @@
     down = lax.psum_scatter(partial_down, "ra", scatter_dimension=0, tiled=True)
     residual = lax.dynamic_slice_in_dim(xfloat, first_row, own_rows, 0)
     mixed = 0.1 * residual + down
-    out_sq = lax.psum(jnp.sum(mixed * mixed, axis=1), "cb")
+    out_sq = jnp.sum(lax.all_gather(jnp.sum(mixed * mixed, axis=1), "cb"), axis=0)
     inv_out = lax.rsqrt(out_sq / D + eps)[:, None]
     return (mixed * inv_out * out_gain.astype(jnp.float32)).astype(jnp.bfloat16)
 

time: 222 us -> 222 us (level)
    psum x1 -> x0, blocking collectives: 5.67 us -> none  [body(): out_sq = lax.psum(jnp.sum(mixed * mixed, axis=1), 'cb')]
    unnamed x0 -> x1, blocking collectives: none -> 5.63 us
where the time goes in v1:
time: 222 us
  waiting for transfers between devices  169 us (76%)
  matrix products  15 us (7%)
  between operations  14.1 us (6%)
  blocking collectives  14 us (6%)
  other arithmetic  8.15 us (4%)
    psum x1, waiting for transfers between devices, body(): total_sq, gate_sum, up_sum = lax.psum((local_sq, gate_part, up_part), 'cb')  104 us
    reduce_scatter x1, waiting for transfers between devices, body(): down = lax.psum_scatter(partial_down, 'ra', scatter_dimension=0, tiled=True)  64.7 us
    psum x1, blocking collectives, body(): total_sq, gate_sum, up_sum = lax.psum((local_sq, gate_part, up_part), 'cb')  8.37 us
    dot_general x1, matrix products, body(): partial_down = jnp.dot(hidden, w_down, preferred_element_type=jnp.float32)  6.83 us
    unnamed x1, blocking collectives  5.63 us
    dot_general x1, matrix products, body(): up_part = jnp.dot(scaled, w_up, preferred_element_type=jnp.float32)  4.74 us
  transfers between devices with their start and end apart: 2, of which 2 were waited for; matrix products, arithmetic and copies ran while one was open for 2% of the time, Pallas kernels for 0%

profile of v1, /device:TPU:0, one launch (start us, length us, event | category | flops | bytes accessed | tf_op | source)
XLA Modules:
  0.0 222.0 jit_solution(258619855604880505)
XLA Ops:
  6.5 0.0 copy-start
  6.5 0.0 all-reduce.4.cloned.1.call-start
  6.5 0.8 convert_element_type.19
  7.4 1.0 copy-done
  8.4 0.0 copy-start.1
  8.4 0.0 copy-start.3
  8.4 4.7 %fusion.1 = f32[512,1408]{1,0:T(8,128)} fusion(bf16[1024,1408]{1,0:T(8,128)(2,1)S(1)} %copy-done, f32[1024]{0:T(1024)S(1)} %convert_element_type.19, bf16[512,1024]{1,0:T(8,128)(2,1)} %param.6), kind=kOutput, calls=%fused_computation.4 | convolution fusion | flops 1477967872 | bytes 6819840 | tf_op jit(solution)/shard_map/dot_general | solution.py:15
  13.1 0.0 copy-done.1
  13.1 0.0 copy-done.3
  13.1 3.5 %fusion.2 = f32[512,1408]{1,0:T(8,128)} fusion(bf16[1024,1408]{1,0:T(8,128)(2,1)S(1)} %copy-done.3, f32[1024]{0:T(1024)S(1)} %convert_element_type.19, bf16[512,1024]{1,0:T(8,128)(2,1)S(1)} %copy-done.1), kind=kOutput, calls=%fused_computation.5 | convolution fusion | flops 1477967872 | bytes 6819840 | tf_op jit(solution)/shard_map/dot_general | solution.py:14
  16.6 0.0 all-reduce.4.cloned.1.call-update
  16.6 0.0 reduce-scatter.2.cloned.1.call-start
  16.6 1.5 multiply_reduce_fusion
  18.1 8.4 %psum.22 = f32[512]{0:T(512)S(1)} all-reduce(f32[512]{0:T(512)S(1)} %multiply_reduce_fusion), channel_id=1, replica_groups=mesh['ra'=8,'cb'=4] {'cb'}, use_global_device_ids=true, to_apply=%region_2.0 | all-reduce | flops 512 | bytes 4096 | tf_op jit(solution)/shard_map/psum | solution.py:16
  26.5 104.0 %all-reduce.4.cloned.1.call-done = (f32[512,1408]{1,0:T(8,128)}, f32[512,1408]{1,0:T(8,128)}) async-done(((f32[512,1408]{1,0:T(8,128)}, f32[512,1408]{1,0:T(8,128)}), (f32[512,1408]{1,0:T(8,128)}, f32[512,1408]{1,0:T(8,128)})) %all-reduce.4.cloned.1.call-update) | async-done | bytes 5767184 | tf_op jit(solution)/shard_map/psum | solution.py:16
  130.5 6.8 %fusion = f32[512,1024]{1,0:T(8,128)} fusion(bf16[1408,1024]{1,0:T(8,128)(2,1)} %param.10, f32[512,1408]{1,0:T(8,128)} %get-tuple-element.5, f32[512,1408]{1,0:T(8,128)} %get-tuple-element.6, f32[512]{0:T(512)S(1)} %add_rsqrt_fusion), kind=kOutput, calls=%fused_computation.3 | convolution fusion | flops 1482162176 | bytes 10749952 | tf_op jit(solution)/shard_map/dot_general | solution.py:19
  137.4 0.0 copy-start.2
  137.4 0.0 copy-start.4
  137.4 0.0 reduce-scatter.2.cloned.1.call-update
  137.4 2.8 %convert_element_type.18 = f32[512,1024]{1,0:T(8,128)} convert(bf16[512,1024]{1,0:T(8,128)(2,1)} %param.6) | non-fusion elementwise | flops 524288 | bytes 3145728 | tf_op jit(solution)/shard_map/convert_element_type | solution.py:11
  140.2 0.0 copy-done.2
  140.2 0.0 copy-done.4
  140.2 0.6 dynamic-slice
  141.5 64.7 %reduce-scatter.2.cloned.1.call-done = f32[64,1024]{1,0:T(8,128)} async-done(((f32[512,1024]{1,0:T(8,128)}), f32[64,1024]{1,0:T(8,128)}) %reduce-scatter.2.cloned.1.call-update) | async-done | bytes 262160 | tf_op jit(solution)/shard_map/reduce_scatter | solution.py:22
  206.2 1.2 multiply_reduce_fusion.1
  207.4 0.2 dynamic-update-slice
  207.6 5.6 %all-reduce = f32[256]{0:T(256)S(1)} all-reduce(f32[256]{0:T(256)S(1)} %dynamic-update-slice), channel_id=2, replica_groups=mesh['ra'=8,'cb'=4] {'cb'}, use_global_device_ids=true, to_apply=%add | all-reduce | flops 256 | bytes 2048
  213.2 0.1 reshape.8
  213.4 1.8 multiply_convert_fusion.5
  (5 shorter events, 0.0 us)
Async XLA Ops:
  6.5 1.8 copy-start
  6.5 124.0 %all-reduce.4.cloned.1.call-start = ((), (), s32[]{:S(2)}) async-start(), calls=%async_computation.2 | async-start | bytes 11534336 | tf_op jit(solution)/shard_map/psum | solution.py:16
  8.4 4.7 %copy-start.1 = (bf16[512,1024]{1,0:T(8,128)(2,1)S(1)}, bf16[512,1024]{1,0:T(8,128)(2,1)}, u32[]{:S(2)}) copy-start(bf16[512,1024]{1,0:T(8,128)(2,1)} %param.6) | copy-start | bytes 3145732
  8.4 4.7 %copy-start.3 = (bf16[1024,1408]{1,0:T(8,128)(2,1)S(1)}, bf16[1024,1408]{1,0:T(8,128)(2,1)}, u32[]{:S(2)}) copy-start(bf16[1024,1408]{1,0:T(8,128)(2,1)} %param.8) | copy-start | bytes 8650756
  16.6 189.6 %reduce-scatter.2.cloned.1.call-start = ((), (), s32[]{:S(2)}) async-start(), calls=%async_computation.1 | async-start | bytes 2359296 | tf_op jit(solution)/shard_map/reduce_scatter | solution.py:22
  137.4 2.9 %copy-start.2 = (bf16[1024]{0:T(1024)(128)(2,1)S(1)}, bf16[1024]{0:T(1024)(128)(2,1)}, u32[]{:S(2)}) copy-start(bf16[1024]{0:T(1024)(128)(2,1)} %param.11) | copy-start | bytes 6148
  137.4 2.9 %copy-start.4 = (u32[32]{0:T(128)S(1)}, u32[32]{0:T(128)}, u32[]{:S(2)}) copy-start(u32[32]{0:T(128)} %constant.29) | copy-start | bytes 388
Sparse Core Ops, SparseCore 0:
  16.7 113.7 all-reduce.3
  137.5 68.6 reduce-scatter.1
